TPU v7x, 32 devices: a whole 2x2x4 slice. The times are simulated.
32 devices in a mesh: fs: 8 (over z, x), tp: 4 (over y, core).
Axes of the slice: x: 2, y: 2, z: 4, core: 2. Of those that a mesh axis runs over, the one named last changes fastest.
Arguments:
- later_input: bfloat16 [6144, 2048], P('fs', 'tp'), may hold values from -6 to 6
- earlier_input: bfloat16 [6144, 2048], P('fs', 'tp'), may hold values from -6 to 6
- cotangent: bfloat16 [6144, 2048], P('fs', 'tp'), may hold values from -6 to 6
- up_weight: bfloat16 [2048, 8192], P('fs', 'tp'), may hold values from -0.125 to 0.125
- down_weight: bfloat16 [8192, 2048], P('tp', 'fs'), may hold values from -0.0625 to 0.0625
- up_running: float32 [2048, 8192], P('fs', 'tp'), may hold values from -6 to 6
- down_running: float32 [2048, 8192], P('fs', 'tp'), may hold values from -6 to 6
Outputs:
- later_output: bfloat16 [6144, 2048], P('fs', 'tp')
- later_preact: bfloat16 [6144, 8192], P('fs', 'tp')
- earlier_grad: bfloat16 [6144, 2048], P('fs', 'tp')
- up_running_out: float32 [2048, 8192], P('fs', 'tp')
- down_running_out: float32 [2048, 8192], P('fs', 'tp')
All inputs are finite; a program needn't handle non-finite values.
Results may differ from a plain program's by a relative error of at most 0.014.
Values may be sent and summed in bfloat16 or wider, within the bound.
A program may use at most 128 MiB of HBM per device.

v0:
```python
import jax
import jax.numpy as jnp
from jax import lax
from jax.sharding import PartitionSpec as P

contract_last = (((1,), (1,)), ((), ()))
contract_first = (((0,), (0,)), ((), ()))


def on_device(
    later_input, earlier_input, cotangent, up_weight, down_weight, up_running, down_running
):
    rows = later_input.shape[0]
    factor = float(rows * lax.axis_size("fs")) ** (-0.5)
    later_full, earlier_full, cot_full = (
        lax.all_gather(later_input, "tp", axis=1, tiled=True),
        lax.all_gather(earlier_input, "tp", axis=1, tiled=True),
        lax.all_gather(cotangent, "tp", axis=1, tiled=True),
    )
    columns = up_weight.shape[1]
    piece = lax.all_gather(up_weight, "fs", axis=0, tiled=True)
    later_up = jnp.dot(later_full, piece, preferred_element_type=jnp.float32)
    earlier_up = jnp.dot(earlier_full, piece, preferred_element_type=jnp.float32)
    later_hidden = jnp.square(jax.nn.relu(later_up)).astype(jnp.bfloat16)
    piece = lax.all_gather(down_weight, "fs", axis=1, tiled=True)
    product = jnp.dot(later_hidden, piece, preferred_element_type=jnp.float32)
    grad = jnp.dot(cot_full, piece.T, preferred_element_type=jnp.float32)
    up_grad = (2.0 * jax.nn.relu(earlier_up) * grad).astype(jnp.bfloat16)
    back_part = lax.dot_general(
        up_grad,
        lax.all_gather(up_weight, "fs", axis=0, tiled=True),
        contract_last,
        preferred_element_type=jnp.float32,
    )
    later_preact = later_up.astype(jnp.bfloat16)
    earlier_hidden = jnp.square(jax.nn.relu(earlier_up)).astype(jnp.bfloat16)
    out_sum, back_sum = (
        lax.psum_scatter(
            product.astype(jnp.bfloat16), "tp", scatter_dimension=1, tiled=True
        ).astype(jnp.float32),
        lax.psum_scatter(
            back_part.astype(jnp.bfloat16), "tp", scatter_dimension=1, tiled=True
        ).astype(jnp.float32),
    )
    summed = lax.psum_scatter(
        jnp.concatenate(
            (
                lax.dot_general(
                    earlier_full, up_grad, contract_first, preferred_element_type=jnp.float32
                ),
                lax.dot_general(
                    cot_full, earlier_hidden, contract_first, preferred_element_type=jnp.float32
                ),
            ),
            axis=1,
        ).astype(jnp.bfloat16),
        "fs",
        scatter_dimension=0,
        tiled=True,
    ).astype(jnp.float32)
    grad_up_sum = summed[:, :columns]
    grad_down_sum = summed[:, columns:]
    return (
        out_sum.astype(jnp.bfloat16),
        later_preact,
        back_sum.astype(jnp.bfloat16),
        up_running + grad_up_sum * factor,
        down_running + grad_down_sum * factor,
    )


def solution(mesh):
    in_specs = (
        P("fs", "tp"),
        P("fs", "tp"),
        P("fs", "tp"),
        P("fs", "tp"),
        P("tp", "fs"),
        P("fs", "tp"),
        P("fs", "tp"),
    )
    out_specs = (P("fs", "tp"), P("fs", "tp"), P("fs", "tp"), P("fs", "tp"), P("fs", "tp"))
    return jax.shard_map(
        on_device, mesh=mesh, in_specs=in_specs, out_specs=out_specs, check_vma=False
    )
```

profile of v0, /device:TPU:0, one launch (start us, length us, event | category | flops | bytes accessed | tf_op | source)
XLA Modules:
  0.0 725.1 jit_solution(515259294564555302)
XLA Ops:
  7.2 0.7 all-gather.12.cloned.1.call-update
  7.9 0.0 all-gather.8.cloned.1.call-start
  7.9 0.7 all-gather.8.cloned.1.call-update
  8.6 0.0 all-gather.14.cloned.1.call-start
  8.7 0.7 all-gather.14.cloned.1.call-update
  9.4 0.5 all-gather.10.cloned.1.call-update
  10.0 0.5 all-gather.6.cloned.1.call-update
  10.5 0.0 reduce-scatter.8.cloned.1.call-start
  10.6 30.2 %all-gather.12.cloned.1.call-done = bf16[768,2048]{1,0:T(8,128)(2,1)} async-done(((bf16[768,512]{1,0:T(8,128)(2,1)}), bf16[768,2048]{1,0:T(8,128)(2,1)}) %all-gather.12.cloned.1.call-update) | async-done | bytes 3145744 | tf_op jit(solution)/shard_map/all_gather | solution.py:17
  40.8 126.6 %all-gather.8.cloned.1.call-done = bf16[2048,2048]{1,0:T(8,128)(2,1)} async-done(((bf16[256,2048]{1,0:T(8,128)(2,1)}), bf16[2048,2048]{1,0:T(8,128)(2,1)}) %all-gather.8.cloned.1.call-update) | async-done | bytes 8388624 | tf_op jit(solution)/shard_map/all_gather | solution.py:21
  167.4 11.6 %fusion.7 = f32[768,2048]{1,0:T(8,128)} fusion(bf16[768,2048]{1,0:T(8,128)(2,1)} %all-gather.12.cloned.1.call-done, bf16[2048,2048]{1,0:T(8,128)(2,1)} %all-gather.8.cloned.1.call-done), kind=kOutput, calls=%fused_computation.17 | convolution fusion | flops 6442450944 | bytes 17825792 | tf_op jit(solution)/shard_map/dot_general | solution.py:23
  179.1 16.6 %all-gather.14.cloned.1.call-done = bf16[768,2048]{1,0:T(8,128)(2,1)} async-done(((bf16[768,512]{1,0:T(8,128)(2,1)}), bf16[768,2048]{1,0:T(8,128)(2,1)}) %all-gather.14.cloned.1.call-update) | async-done | bytes 3145744 | tf_op jit(solution)/shard_map/all_gather | solution.py:18
  195.7 126.9 %all-gather.10.cloned.1.call-done = bf16[2048,2048]{1,0:T(8,128)(2,1)} async-done(((bf16[2048,256]{1,0:T(8,128)(2,1)}), bf16[2048,2048]{1,0:T(8,128)(2,1)}) %all-gather.10.cloned.1.call-update) | async-done | bytes 8388624 | tf_op jit(solution)/shard_map/all_gather | solution.py:25
  322.6 11.8 %multiply_convert_fusion.1 = bf16[768,2048]{1,0:T(8,128)(2,1)S(1)} fusion(f32[768,2048]{1,0:T(8,128)} %fusion.7, bf16[768,2048]{1,0:T(8,128)(2,1)} %all-gather.14.cloned.1.call-done, bf16[2048,2048]{1,0:T(8,128)(2,1)} %all-gather.10.cloned.1.call-done), kind=kOutput, calls=%fused_computation.4 | convolution fusion | flops 6448742400 | bytes 20971520 | tf_op jit(solution)/shard_map/dot_general | solution.py:27
  334.4 7.0 convert_bitcast_fusion.1
  341.4 10.0 %convert_bitcast_fusion = bf16[2048,2048]{0,1:T(8,128)(2,1)S(1)} fusion(bf16[768,2048]{1,0:T(8,128)(2,1)S(1)} %copy-done.3, f32[768,2048]{1,0:T(8,128)} %fusion.7), kind=kOutput, calls=%fused_computation.1 | convolution fusion | flops 6451363840 | bytes 17825792 | tf_op jit(solution)/shard_map/dot_general | solution.py:51
  351.4 7.5 %pad_maximum_fusion = bf16[2048,4096]{0,1:T(8,128)(2,1)} fusion(bf16[2048,2048]{0,1:T(8,128)(2,1)S(1)} %convert_bitcast_fusion, bf16[2048,2048]{0,1:T(8,128)(2,1)S(1)} %convert_bitcast_fusion.1), kind=kLoop, calls=%fused_computation | loop fusion | flops 33554432 | bytes 33554432 | tf_op jit(solution)/shard_map/concatenate | solution.py:46
  358.9 0.0 reduce-scatter.4.cloned.1.call-start
  359.0 11.2 %fusion.6 = (bf16[768,2048]{1,0:T(8,128)(2,1)}, f32[768,2048]{1,0:T(8,128)S(1)}) fusion(bf16[768,2048]{1,0:T(8,128)(2,1)} %all-gather.6.cloned.1.call-done, bf16[2048,2048]{1,0:T(8,128)(2,1)} %all-gather.8.cloned.1.call-done), kind=kOutput, calls=%fused_computation.16 | convolution fusion | flops 6444023808 | bytes 20971520 | tf_op jit(solution)/shard_map/dot_general | solution.py:22
  370.1 10.4 %convolution_convert_fusion.1 = bf16[768,2048]{1,0:T(8,128)(2,1)} fusion(bf16[2048,2048]{1,0:T(8,128)(2,1)} %all-gather.10.cloned.1.call-done, f32[768,2048]{1,0:T(8,128)S(1)} %get-tuple-element.13), kind=kOutput, calls=%fused_computation.7 | convolution fusion | flops 6448742400 | bytes 17825792 | tf_op jit(solution)/shard_map/dot_general | solution.py:26
  380.6 0.0 reduce-scatter.6.cloned.1.call-start
  380.6 10.5 %convolution_convert_fusion = bf16[768,2048]{1,0:T(8,128)(2,1)} fusion(bf16[768,2048]{1,0:T(8,128)(2,1)S(1)} %copy-done.5, bf16[2048,2048]{1,0:T(8,128)(2,1)} %all-gather.8.cloned.1.call-done), kind=kOutput, calls=%fused_computation.6 | convolution fusion | flops 6444023808 | bytes 14680064 | tf_op jit(solution)/shard_map/dot_general | solution.py:29
  391.2 1.9 copy.13
  393.1 2.9 copy.12
  396.0 241.4 %reduce-scatter.8.cloned.1.call-done = bf16[256,4096]{0,1:T(8,128)(2,1)} async-done(((bf16[2048,4096]{0,1:T(8,128)(2,1)}), bf16[256,4096]{0,1:T(8,128)(2,1)}) %reduce-scatter.8.cloned.1.call-update) | async-done | bytes 2097168 | tf_op jit(solution)/shard_map/reduce_scatter | solution.py:45
  637.4 2.1 convert_element_type.32
  639.5 0.1 copy-done
  639.6 2.8 fusion.2
  642.4 3.0 copy.14
  645.5 1.8 copy.15
  647.3 30.1 %reduce-scatter.4.cloned.1.call-done = bf16[768,512]{1,0:T(8,128)(2,1)} async-done(((bf16[768,2048]{1,0:T(8,128)(2,1)}), bf16[768,512]{1,0:T(8,128)(2,1)}) %reduce-scatter.4.cloned.1.call-update) | async-done | bytes 786448 | tf_op jit(solution)/shard_map/reduce_scatter | solution.py:38
  677.4 40.9 %reduce-scatter.6.cloned.1.call-done = bf16[768,512]{1,0:T(8,128)(2,1)} async-done(((bf16[768,2048]{1,0:T(8,128)(2,1)}), bf16[768,512]{1,0:T(8,128)(2,1)}) %reduce-scatter.6.cloned.1.call-update) | async-done | bytes 786448 | tf_op jit(solution)/shard_map/reduce_scatter | solution.py:41
  (18 shorter events, 0.2 us)
Async XLA Ops:
  7.2 33.6 %all-gather.12.cloned.1.call-start = ((), (), s32[]{:S(2)}) async-start(), calls=%async_computation.7 | async-start | bytes 3932160 | tf_op jit(solution)/shard_map/all_gather | solution.py:17
  7.9 159.5 %all-gather.8.cloned.1.call-start = ((), (), s32[]{:S(2)}) async-start(), calls=%async_computation.4 | async-start | bytes 9437184 | tf_op jit(solution)/shard_map/all_gather | solution.py:21
  8.6 187.1 %all-gather.14.cloned.1.call-start = ((), (), s32[]{:S(2)}) async-start(), calls=%async_computation.8 | async-start | bytes 3932160 | tf_op jit(solution)/shard_map/all_gather | solution.py:18
  9.4 313.2 %all-gather.10.cloned.1.call-start = ((), (), s32[]{:S(2)}) async-start(), calls=%async_computation.5 | async-start | bytes 9437184 | tf_op jit(solution)/shard_map/all_gather | solution.py:25
  10.0 349.0 %all-gather.6.cloned.1.call-start = ((), (), s32[]{:S(2)}) async-start(), calls=%async_computation.3 | async-start | bytes 3932160 | tf_op jit(solution)/shard_map/all_gather | solution.py:16
  10.5 626.9 %reduce-scatter.8.cloned.1.call-start = ((), (), s32[]{:S(2)}) async-start(), calls=%async_computation.10 | async-start | bytes 18874368 | tf_op jit(solution)/shard_map/reduce_scatter | solution.py:45
  179.1 155.3 %copy-start.2 = (bf16[768,2048]{1,0:T(8,128)(2,1)S(1)}, bf16[768,2048]{1,0:T(8,128)(2,1)}, u32[]{:S(2)}) copy-start(bf16[768,2048]{1,0:T(8,128)(2,1)} %all-gather.12.cloned.1.call-done) | copy-start | bytes 9437188
  334.4 7.0 copy-start.4
  334.4 7.0 copy-start.3
  358.9 318.5 %reduce-scatter.4.cloned.1.call-start = ((), (), s32[]{:S(2)}) async-start(), calls=%async_computation.6 | async-start | bytes 3932160 | tf_op jit(solution)/shard_map/reduce_scatter | solution.py:38
  370.1 10.5 %copy-start.5 = (bf16[768,2048]{1,0:T(8,128)(2,1)S(1)}, bf16[768,2048]{1,0:T(8,128)(2,1)}, u32[]{:S(2)}) copy-start(bf16[768,2048]{1,0:T(8,128)(2,1)} %copy-done.4) | copy-start | bytes 9437188
  380.6 337.6 %reduce-scatter.6.cloned.1.call-start = ((), (), s32[]{:S(2)}) async-start(), calls=%async_computation.9 | async-start | bytes 3932160 | tf_op jit(solution)/shard_map/reduce_scatter | solution.py:41
  637.4 2.2 copy-start
  642.4 3.0 copy-start.1
Sparse Core Ops, SparseCore 0:
  9.5 31.2 all-gather.11
  42.9 124.4 all-gather.7
  169.0 26.6 all-gather.13
  197.6 124.9 all-gather.9
  324.0 26.6 all-gather.5
  359.0 278.3 reduce-scatter.7
  640.5 36.8 reduce-scatter.3
  680.5 37.7 reduce-scatter.5
where the time goes:
time: 725 us
  waiting for transfers between devices  616 us (85%)
  matrix products  72.5 us (10%)
  between operations  14.2 us (2%)
  other arithmetic  12.3 us (2%)
  local copies, waits for them, and re-layouts  9.82 us (1%)
    reduce_scatter x1, waiting for transfers between devices, on_device(): lax.psum_scatter(jnp.concatenate((lax.dot_general(earlier_full, up_grad,...  241 us
    all_gather x1, waiting for transfers between devices, on_device(): piece = lax.all_gather(down_weight, 'fs', axis=1, tiled=True)  127 us
    all_gather x1, waiting for transfers between devices, on_device(): piece = lax.all_gather(up_weight, 'fs', axis=0, tiled=True)  127 us
    reduce_scatter x1, waiting for transfers between devices, on_device(): lax.psum_scatter(back_part.astype(jnp.bfloat16), 'tp', scatter_dimension=...  40.9 us
    all_gather x1, waiting for transfers between devices, on_device(): lax.all_gather(earlier_input, 'tp', axis=1, tiled=True)  30.2 us
    reduce_scatter x1, waiting for transfers between devices, on_device(): lax.psum_scatter(product.astype(jnp.bfloat16), 'tp', scatter_dimension=1,...  30.1 us
    all_gather x1, waiting for transfers between devices, on_device(): lax.all_gather(cotangent, 'tp', axis=1, tiled=True)  16.6 us
  transfers between devices with their start and end apart: 8, of which 7 were waited for; matrix products, arithmetic and copies ran while one was open for 13% of the time, Pallas kernels for 0%

commit v1 on v0

--- a/solution.py
+++ b/solution.py
@@ -18,7 +18,10 @@
         lax.all_gather(cotangent, "tp", axis=1, tiled=True),
     )
     columns = up_weight.shape[1]
-    piece = lax.all_gather(up_weight, "fs", axis=0, tiled=True)
+    size = lax.axis_size("fs")
+    blocks = jnp.stack([up_weight for _ in range(size)])
+    blocks = lax.all_to_all(blocks, "fs", split_axis=0, concat_axis=0)
+    piece = jnp.concatenate(blocks, axis=0)
     later_up = jnp.dot(later_full, piece, preferred_element_type=jnp.float32)
     earlier_up = jnp.dot(earlier_full, piece, preferred_element_type=jnp.float32)
     later_hidden = jnp.square(jax.nn.relu(later_up)).astype(jnp.bfloat16)

time: 725 us -> 832 us (1.15)
  waiting for transfers between devices: 616 us -> 708 us
    all_to_all x0 -> x1, waiting for transfers between devices: none -> 260 us  [on_device(): blocks = lax.all_to_all(blocks, 'fs', split_axis=0, concat_axis=0)]
    all_gather x1, waiting for transfers between devices: 127 us -> 0.01 us  [on_device(): piece = lax.all_gather(down_weight, 'fs', axis=1, tiled=True)]
    all_gather x1, waiting for transfers between devices: 127 us -> 90.2 us  [on_device(): lax.all_gather(up_weight, 'fs', axis=0, tiled=True)]
    reduce_scatter x1, waiting for transfers between devices: 241 us -> 267 us  [on_device(): lax.psum_scatter(jnp.concatenate((lax.dot_general(earlier_full, up_grad,...]
    all_gather x1, waiting for transfers between devices: 16.6 us -> 0.01 us  [on_device(): lax.all_gather(cotangent, 'tp', axis=1, tiled=True)]
    all_gather x1, waiting for transfers between devices: 30.2 us -> 17.4 us  [on_device(): lax.all_gather(earlier_input, 'tp', axis=1, tiled=True)]
  transfers between devices with their start and end apart: 8 -> 9, of which waited for: 7 -> 6; matrix products, arithmetic and copies ran while one was open for 13% -> 12% of each run, Pallas kernels for 0% -> 0%
where the time goes in v1:
time: 832 us
  waiting for transfers between devices  708 us (85%)
  matrix products  73.3 us (9%)
  local copies, waits for them, and re-layouts  16.3 us (2%)
  between operations  14.2 us (2%)
  other arithmetic  12.2 us (1%)
    reduce_scatter x1, waiting for transfers between devices, on_device(): lax.psum_scatter(jnp.concatenate((lax.dot_general(earlier_full, up_grad,...  267 us
    all_to_all x1, waiting for transfers between devices, on_device(): blocks = lax.all_to_all(blocks, 'fs', split_axis=0, concat_axis=0)  260 us
    all_gather x1, waiting for transfers between devices, on_device(): lax.all_gather(up_weight, 'fs', axis=0, tiled=True)  90.2 us
    reduce_scatter x1, waiting for transfers between devices, on_device(): lax.psum_scatter(back_part.astype(jnp.bfloat16), 'tp', scatter_dimension=...  40.9 us
    reduce_scatter x1, waiting for transfers between devices, on_device(): lax.psum_scatter(product.astype(jnp.bfloat16), 'tp', scatter_dimension=1,...  29.3 us
    all_gather x1, waiting for transfers between devices, on_device(): lax.all_gather(earlier_input, 'tp', axis=1, tiled=True)  17.4 us
  transfers between devices with their start and end apart: 9, of which 6 were waited for; matrix products, arithmetic and copies ran while one was open for 12% of the time, Pallas kernels for 0%

profile of v1, /device:TPU:0, one launch (start us, length us, event | category | flops | bytes accessed | tf_op | source)
XLA Modules:
  0.0 832.0 jit_solution(9401762031708735880)
XLA Ops:
  7.2 0.7 all-gather.10.cloned.1.call-update
  7.9 0.0 all-gather.12.cloned.1.call-start
  7.9 0.7 all-gather.12.cloned.1.call-update
  8.7 0.7 all-gather.8.cloned.1.call-update
  9.4 5.5 stack.2
  14.9 7.3 all-to-all-start
  22.3 0.5 all-gather.6.cloned.1.call-update
  22.8 0.5 all-gather.14.cloned.1.call-update
  23.4 0.0 reduce-scatter.8.cloned.1.call-start
  23.4 17.4 %all-gather.10.cloned.1.call-done = bf16[768,2048]{1,0:T(8,128)(2,1)} async-done(((bf16[768,512]{1,0:T(8,128)(2,1)}), bf16[768,2048]{1,0:T(8,128)(2,1)}) %all-gather.10.cloned.1.call-update) | async-done | bytes 3145744 | tf_op jit(solution)/shard_map/all_gather | solution.py:17
  40.8 260.4 %all-to-all-done = bf16[8,256,2048]{2,1,0:T(8,128)(2,1)} async-done(((bf16[8,256,2048]{2,1,0:T(8,128)(2,1)}), bf16[8,256,2048]{2,1,0:T(8,128)(2,1)}, u32[]{:S(2)}, u32[]{:S(2)}) %all-to-all-start) | async-done | bytes 8388640 | tf_op jit(solution)/shard_map/all_to_all | solution.py:23
  301.2 11.7 %fusion.7 = f32[768,2048]{1,0:T(8,128)} fusion(bf16[768,2048]{1,0:T(8,128)(2,1)} %all-gather.10.cloned.1.call-done, bf16[2048,2048]{1,0:T(8,128)(2,1)} %bitcast), kind=kOutput, calls=%fused_computation.17 | convolution fusion | flops 6442450944 | bytes 17825792 | tf_op jit(solution)/shard_map/dot_general | solution.py:26
  312.9 12.8 %multiply_convert_fusion.1 = bf16[768,2048]{1,0:T(8,128)(2,1)S(1)} fusion(f32[768,2048]{1,0:T(8,128)} %fusion.7, bf16[768,2048]{1,0:T(8,128)(2,1)} %all-gather.12.cloned.1.call-done, bf16[2048,2048]{1,0:T(8,128)(2,1)} %all-gather.8.cloned.1.call-done), kind=kOutput, calls=%fused_computation.4 | convolution fusion | flops 6448742400 | bytes 20971520 | tf_op jit(solution)/shard_map/dot_general | solution.py:30
  325.7 7.0 convert_bitcast_fusion.1
  332.7 10.0 %convert_bitcast_fusion = bf16[2048,2048]{0,1:T(8,128)(2,1)S(1)} fusion(bf16[768,2048]{1,0:T(8,128)(2,1)S(1)} %copy-done.2, f32[768,2048]{1,0:T(8,128)} %fusion.7), kind=kOutput, calls=%fused_computation.1 | convolution fusion | flops 6451363840 | bytes 17825792 | tf_op jit(solution)/shard_map/dot_general | solution.py:54
  342.7 7.5 pad_maximum_fusion
  350.3 0.0 reduce-scatter.4.cloned.1.call-start
  350.3 11.2 %fusion.6 = (bf16[768,2048]{1,0:T(8,128)(2,1)}, f32[768,2048]{1,0:T(8,128)S(1)}) fusion(bf16[768,2048]{1,0:T(8,128)(2,1)} %all-gather.6.cloned.1.call-done, bf16[2048,2048]{1,0:T(8,128)(2,1)} %bitcast), kind=kOutput, calls=%fused_computation.16 | convolution fusion | flops 6444023808 | bytes 20971520 | tf_op jit(solution)/shard_map/dot_general | solution.py:25
  361.5 10.4 %convolution_convert_fusion.1 = bf16[768,2048]{1,0:T(8,128)(2,1)} fusion(bf16[2048,2048]{1,0:T(8,128)(2,1)} %all-gather.8.cloned.1.call-done, f32[768,2048]{1,0:T(8,128)S(1)} %get-tuple-element.13), kind=kOutput, calls=%fused_computation.7 | convolution fusion | flops 6448742400 | bytes 17825792 | tf_op jit(solution)/shard_map/dot_general | solution.py:29
  372.0 0.0 reduce-scatter.6.cloned.1.call-start
  372.0 90.2 %all-gather.14.cloned.1.call-done = bf16[2048,2048]{1,0:T(8,128)(2,1)} async-done(((bf16[256,2048]{1,0:T(8,128)(2,1)}), bf16[2048,2048]{1,0:T(8,128)(2,1)}) %all-gather.14.cloned.1.call-update) | async-done | bytes 8388624 | tf_op jit(solution)/shard_map/all_gather | solution.py:34
  462.3 10.3 %convolution_convert_fusion = bf16[768,2048]{1,0:T(8,128)(2,1)} fusion(bf16[768,2048]{1,0:T(8,128)(2,1)S(1)} %copy-done.4, bf16[2048,2048]{1,0:T(8,128)(2,1)} %all-gather.14.cloned.1.call-done), kind=kOutput, calls=%fused_computation.6 | convolution fusion | flops 6444023808 | bytes 14680064 | tf_op jit(solution)/shard_map/dot_general | solution.py:32
  472.5 1.9 copy.13
  474.5 2.9 copy.12
  477.4 267.0 %reduce-scatter.8.cloned.1.call-done = bf16[256,4096]{0,1:T(8,128)(2,1)} async-done(((bf16[2048,4096]{0,1:T(8,128)(2,1)}), bf16[256,4096]{0,1:T(8,128)(2,1)}) %reduce-scatter.8.cloned.1.call-update) | async-done | bytes 2097168 | tf_op jit(solution)/shard_map/reduce_scatter | solution.py:48
  744.4 2.1 convert_element_type.32
  746.4 0.1 copy-done
  746.6 2.7 fusion.2
  749.3 2.9 copy.14
  752.1 2.9 copy.15
  755.0 29.3 %reduce-scatter.4.cloned.1.call-done = bf16[768,512]{1,0:T(8,128)(2,1)} async-done(((bf16[768,2048]{1,0:T(8,128)(2,1)}), bf16[768,512]{1,0:T(8,128)(2,1)}) %reduce-scatter.4.cloned.1.call-update) | async-done | bytes 786448 | tf_op jit(solution)/shard_map/reduce_scatter | solution.py:41
  784.3 40.9 %reduce-scatter.6.cloned.1.call-done = bf16[768,512]{1,0:T(8,128)(2,1)} async-done(((bf16[768,2048]{1,0:T(8,128)(2,1)}), bf16[768,512]{1,0:T(8,128)(2,1)}) %reduce-scatter.6.cloned.1.call-update) | async-done | bytes 786448 | tf_op jit(solution)/shard_map/reduce_scatter | solution.py:44
  (19 shorter events, 0.2 us)
Async XLA Ops:
  7.2 33.6 %all-gather.10.cloned.1.call-start = ((), (), s32[]{:S(2)}) async-start(), calls=%async_computation.7 | async-start | bytes 3932160 | tf_op jit(solution)/shard_map/all_gather | solution.py:17
  7.9 305.0 %all-gather.12.cloned.1.call-start = ((), (), s32[]{:S(2)}) async-start(), calls=%async_computation.8 | async-start | bytes 3932160 | tf_op jit(solution)/shard_map/all_gather | solution.py:18
  8.6 304.3 %all-gather.8.cloned.1.call-start = ((), (), s32[]{:S(2)}) async-start(), calls=%async_computation.5 | async-start | bytes 9437184 | tf_op jit(solution)/shard_map/all_gather | solution.py:28
  14.9 286.2 %all-to-all-start = ((bf16[8,256,2048]{2,1,0:T(8,128)(2,1)}), bf16[8,256,2048]{2,1,0:T(8,128)(2,1)}, u32[]{:S(2)}, u32[]{:S(2)}) async-start(bf16[8,256,2048]{2,1,0:T(8,128)(2,1)} %stack.2), calls=%async_computation | async-start | bytes 16777216 | tf_op jit(solution)/shard_map/all_to_all | solution.py:23
  22.2 328.1 %all-gather.6.cloned.1.call-start = ((), (), s32[]{:S(2)}) async-start(), calls=%async_computation.4 | async-start | bytes 3932160 | tf_op jit(solution)/shard_map/all_gather | solution.py:16
  22.8 439.5 %all-gather.14.cloned.1.call-start = ((), (), s32[]{:S(2)}) async-start(), calls=%async_computation.9 | async-start | bytes 9437184 | tf_op jit(solution)/shard_map/all_gather | solution.py:34
  23.4 721.0 %reduce-scatter.8.cloned.1.call-start = ((), (), s32[]{:S(2)}) async-start(), calls=%async_computation.11 | async-start | bytes 18874368 | tf_op jit(solution)/shard_map/reduce_scatter | solution.py:48
  312.9 12.8 %copy-start.1 = (bf16[768,2048]{1,0:T(8,128)(2,1)S(1)}, bf16[768,2048]{1,0:T(8,128)(2,1)}, u32[]{:S(2)}) copy-start(bf16[768,2048]{1,0:T(8,128)(2,1)} %all-gather.10.cloned.1.call-done) | copy-start | bytes 9437188
  325.7 7.0 copy-start.3
  325.7 7.0 copy-start.2
  350.3 434.1 %reduce-scatter.4.cloned.1.call-start = ((), (), s32[]{:S(2)}) async-start(), calls=%async_computation.6 | async-start | bytes 3932160 | tf_op jit(solution)/shard_map/reduce_scatter | solution.py:41
  361.5 100.7 %copy-start.4 = (bf16[768,2048]{1,0:T(8,128)(2,1)S(1)}, bf16[768,2048]{1,0:T(8,128)(2,1)}, u32[]{:S(2)}) copy-start(bf16[768,2048]{1,0:T(8,128)(2,1)} %copy-done.3) | copy-start | bytes 9437188
  372.0 453.2 %reduce-scatter.6.cloned.1.call-start = ((), (), s32[]{:S(2)}) async-start(), calls=%async_computation.10 | async-start | bytes 3932160 | tf_op jit(solution)/shard_map/reduce_scatter | solution.py:44
  744.4 2.2 copy-start
Sparse Core Ops, SparseCore 0:
  9.5 31.2 all-gather.9
  42.4 28.4 all-gather.11
  73.0 233.8 all-gather.7
  308.2 27.4 all-gather.5
  337.8 124.4 all-gather.13
  465.9 278.4 reduce-scatter.7
  747.5 36.8 reduce-scatter.3
  787.4 37.7 reduce-scatter.5
